TPU v7x, 32 devices: a whole 2x2x4 slice. The times are simulated.
32 devices in a mesh: ep: 4 (over y, x), tp: 8 (over z, core).
Axes of the slice: x: 2, y: 2, z: 4, core: 2. Of those that a mesh axis runs over, the one named last changes fastest.
Arguments:
- query_heads_rows: bfloat16 [2048, 2048], P('ep', 'tp'), may hold values from -9 to 9
- key_heads_rows: bfloat16 [2048, 2048], P('ep', 'tp'), may hold values from -9 to 9
- value_heads_rows: bfloat16 [2048, 2048], P('ep', 'tp'), may hold values from -6 to 6
- write_strength_logit: bfloat16 [16, 2048], P('tp', 'ep'), may hold values from -3.5 to -1
- decay_preactivation: bfloat16 [16, 2048], P('tp', 'ep'), may hold values from -5 to 5
- head_decay_logarithm: float32 [16], P('tp'), may hold values from -20 to -3
- extra_log_decay: float32 [16, 2048], P('tp', 'ep'), may hold values from -0.7 to 0
- output_weight: bfloat16 [2048, 2048], P('tp'), may hold values from -2 to 2
- second_batch_tokens: bfloat16 [4096, 2048], P(('ep', 'tp')), may hold values from -6 to 6
- expert_norm_scale: float32 [2048], replicated, may hold values from 0.1 to 1.9
- expert_choice_index: int32 [4096, 2], P(('ep', 'tp')), may hold values from 0 to 15, as said below
- group_router_weight: float32 [4096], P(('ep', 'tp')), may hold values from 0.25 to 1
- expert_logit_difference: float32 [4096], P(('ep', 'tp')), may hold values from -8 to 8
- expert_gate_weight: bfloat16 [16, 1024, 2048], P('ep', 'tp'), may hold values from -0.125 to 0.125
- expert_up_weight: bfloat16 [16, 1024, 2048], P('ep', 'tp'), may hold values from -0.125 to 0.125
- expert_down_weight: bfloat16 [16, 1024, 2048], P('ep', 'tp'), may hold values from -0.375 to 0.375
Outputs:
- mixer_output_first: bfloat16 [2048, 2048], P(('ep', 'tp'))
- expert_out: bfloat16 [4096, 2048], P(('ep', 'tp'))
Inputs may be any that keep to these rules, and one draw needn't show every extreme that they name: `expert_choice_index`: each row names two different experts of one group, the experts a * 4 to a * 4 + 3 for some a. In the rows of one device (aligned blocks of 128 rows) no expert is named more than 32 times, and in every device's rows some expert is named exactly 32 times.
All inputs are finite; a program needn't handle non-finite values.
Results may differ from a plain program's by a relative error of at most 0.018.
Values may be sent and summed in bfloat16 or wider, within the bound.
A program may use at most 128 MiB of HBM per device.

v0:
```python
import jax
import jax.numpy as jnp
from jax import lax
from jax.sharding import PartitionSpec as P

DK = 128
DV = 128
BLOCK = 64
CAP = 32
EXPERTS = 16
TOPK = 2
precise_setting = lax.Precision.HIGHEST
norm_eps = 1e-06


def prefix(value, axis, join, neutral):
    count, mine = (lax.axis_size(axis), lax.axis_index(axis))
    pieces = jax.tree.map(lambda part: lax.all_gather(part, axis), value)
    subtotal = jax.tree.map(
        lambda part, zero: jnp.full_like(part, 0) + jnp.asarray(zero, part.dtype), value, neutral
    )

    def step(position, subtotal):
        longer = join(subtotal, jax.tree.map(lambda part: part[position], pieces))
        return jax.tree.map(lambda new, old: jnp.where(position < mine, new, old), longer, subtotal)

    return lax.fori_loop(0, count - 1, step, subtotal)


def unit_rows(matrix):
    return matrix * lax.rsqrt(jnp.sum(matrix * matrix, axis=-1, keepdims=True) + norm_eps)


def block_terms(query_block, key_block, value_block, decay_logarithm, strength):
    span_len = query_block.shape[2]
    dim_value = value_block.shape[-1]
    cumulative = jnp.cumsum(decay_logarithm, axis=-1)
    within = jnp.tril(jnp.ones((span_len, span_len), bool))
    strict = jnp.tril(jnp.ones((span_len, span_len), bool), -1)
    spread = cumulative[..., :, None] - cumulative[..., None, :]
    decayed = jnp.where(within, jnp.exp(jnp.where(within, spread, 0.0)), 0.0)
    weighted = key_block * strength[..., None]
    lower_part = jnp.where(
        strict,
        jnp.einsum("hnid,hnjd->hnij", weighted, key_block, precision=precise_setting) * decayed,
        0.0,
    )
    system = lower_part + jnp.eye(span_len, dtype=jnp.float32)
    rhs_cols = jnp.concatenate(
        [value_block * strength[..., None], weighted * jnp.exp(cumulative)[..., None]], axis=-1
    )
    solved = jax.scipy.linalg.solve_triangular(system, rhs_cols, lower=True, unit_diagonal=True)
    updated_values = solved[..., :dim_value]
    delta_corrections = solved[..., dim_value:]
    scores = jnp.where(
        within,
        jnp.einsum("hnid,hnjd->hnij", query_block, key_block, precision=precise_setting) * decayed,
        0.0,
    )
    decayed_queries = query_block * jnp.exp(cumulative)[..., None]
    decayed_keys = key_block * jnp.exp(cumulative[..., -1:] - cumulative)[..., None]
    block_retention = jnp.exp(cumulative[..., -1])
    return (
        decayed_queries,
        decayed_keys,
        updated_values,
        delta_corrections,
        scores,
        block_retention,
    )


def carry_step(recurrent_state, inputs):
    decayed_queries, decayed_keys, updated_values, delta_corrections, scores, block_retention = (
        inputs
    )
    value_updates = updated_values - jnp.einsum(
        "jdb,jbu->jdu", delta_corrections, recurrent_state, precision=precise_setting
    )
    final_output = jnp.einsum(
        "jdb,jbu->jdu", decayed_queries, recurrent_state, precision=precise_setting
    )
    final_output = final_output + jnp.einsum(
        "hcj,hjv->hcv", scores, value_updates, precision=precise_setting
    )
    recurrent_state = recurrent_state * block_retention[:, None, None] + jnp.einsum(
        "rpq,rpd->rqd", decayed_keys, value_updates, precision=precise_setting
    )
    return (recurrent_state, final_output)


def compose(earlier, latter):
    joined_map = jnp.einsum("hij,hjk->hik", latter[0], earlier[0], precision=precise_setting)
    joined_state = (
        jnp.einsum("hij,hjv->hiv", latter[0], earlier[1], precision=precise_setting) + latter[1]
    )
    return (joined_map, joined_state)


def shards(
    query_heads_rows,
    key_heads_rows,
    value_heads_rows,
    write_strength_logit,
    decay_preactivation,
    head_decay_logarithm,
    extra_log_decay,
    output_weight,
    second_batch_tokens,
    expert_norm_scale,
    expert_choice_index,
    group_router_weight,
    expert_logit_difference,
    expert_gate_weight,
    expert_up_weight,
    expert_down_weight,
):
    length = query_heads_rows.shape[0]
    local_heads = head_decay_logarithm.shape[0]
    blocks = length // BLOCK
    width_model = output_weight.shape[1]

    def heads_first(matrix):
        spread_out = matrix.astype(jnp.float32).reshape(length, local_heads, -1).transpose(1, 0, 2)
        return spread_out.reshape(local_heads, blocks, BLOCK, -1)

    query_block = unit_rows(heads_first(query_heads_rows)) * DK ** (-0.5)
    key_block = unit_rows(heads_first(key_heads_rows))
    value_block = heads_first(value_heads_rows)
    strength = jax.nn.sigmoid(write_strength_logit.astype(jnp.float32)).reshape(
        local_heads, blocks, BLOCK
    )
    decay_logarithm = (
        -jnp.exp(head_decay_logarithm)[:, None]
        * jax.nn.softplus(decay_preactivation.astype(jnp.float32))
        + extra_log_decay
    )
    decay_logarithm = decay_logarithm.reshape(local_heads, blocks, BLOCK)
    decayed_queries, decayed_keys, updated_values, delta_corrections, scores, block_retention = (
        block_terms(query_block, key_block, value_block, decay_logarithm, strength)
    )
    fresh_wide = jnp.concatenate(
        [updated_values, jnp.zeros(updated_values.shape[:-1] + (DK,), jnp.float32)], axis=-1
    )
    inputs = tuple(
        (
            jnp.moveaxis(term, 1, 0)
            for term in (
                decayed_queries,
                decayed_keys,
                fresh_wide,
                delta_corrections,
                scores,
                block_retention,
            )
        )
    )
    identity_map = jnp.broadcast_to(jnp.eye(DK, dtype=jnp.float32), (local_heads, DK, DK))
    start_memory = jnp.concatenate(
        [jnp.zeros((local_heads, DK, DV), jnp.float32), identity_map], axis=-1
    )
    end_memory, outputs = lax.scan(carry_step, start_memory, inputs)
    local_output = outputs[..., :DV]
    projection_matrix = outputs[..., DV:]
    carried_end = end_memory[..., :DV]
    transfer = end_memory[..., DV:]
    _, incoming_rows = prefix(
        (transfer, carried_end), "ep", compose, (identity_map, jnp.zeros_like(carried_end))
    )
    attention_result = local_output + jnp.einsum(
        "xtyg,tgd->xtyd", projection_matrix, incoming_rows, precision=precise_setting
    )
    attn_rows = (
        attention_result.transpose(0, 2, 1, 3)
        .reshape(length, local_heads * DV)
        .astype(jnp.bfloat16)
    )
    summed = lax.psum_scatter(
        jnp.dot(attn_rows, output_weight, preferred_element_type=jnp.float32).astype(jnp.bfloat16),
        "tp",
        scatter_dimension=0,
        tiled=True,
    )
    widened = second_batch_tokens.astype(jnp.float32)
    normed = (
        widened
        * lax.rsqrt(jnp.mean(widened * widened, axis=-1, keepdims=True) + norm_eps)
        * expert_norm_scale
    ).astype(jnp.bfloat16)
    own_tokens = second_batch_tokens.shape[0]
    ep_count = lax.axis_size("ep")
    local_experts = EXPERTS // ep_count
    flat_ids = expert_choice_index.reshape(-1)
    one_hot = (flat_ids[:, None] == jnp.arange(EXPERTS, dtype=jnp.int32)[None, :]).astype(jnp.int32)
    slot_rank = jnp.sum((jnp.cumsum(one_hot, axis=0) - one_hot) * one_hot, axis=1)
    slot_index = flat_ids * CAP + slot_rank
    copy_token = jnp.arange(flat_ids.shape[0], dtype=jnp.int32) // TOPK
    slot_token = jnp.full((EXPERTS * CAP,), own_tokens, jnp.int32).at[slot_index].set(copy_token)
    outgoing = jnp.take(normed, slot_token, axis=0, mode="fill", fill_value=0).reshape(
        ep_count, local_experts, CAP, width_model
    )
    arrived = lax.all_to_all(outgoing, "ep", split_axis=0, concat_axis=0, tiled=True)
    gate_piece = lax.all_gather(expert_gate_weight, "tp", axis=1, tiled=True)
    up_piece = lax.all_gather(expert_up_weight, "tp", axis=1, tiled=True)
    down_piece = lax.all_gather(expert_down_weight, "tp", axis=1, tiled=True)
    gating = jnp.einsum("secd,efd->secf", arrived, gate_piece, preferred_element_type=jnp.float32)
    upward = jnp.einsum("secd,efd->secf", arrived, up_piece, preferred_element_type=jnp.float32)
    hidden = (jax.nn.silu(gating) * upward).astype(jnp.bfloat16)
    produced = jnp.einsum("secf,efd->secd", hidden, down_piece, preferred_element_type=jnp.float32)
    returned = lax.all_to_all(
        produced.astype(jnp.bfloat16), "ep", split_axis=0, concat_axis=0, tiled=True
    )
    flat_results = returned.reshape(EXPERTS * CAP, width_model)
    picked = (
        jnp.take(flat_results, slot_index, axis=0)
        .reshape(own_tokens, TOPK, width_model)
        .astype(jnp.float32)
    )
    leading = jax.nn.sigmoid(expert_logit_difference)
    mixing = group_router_weight[:, None] * jnp.stack([leading, 1.0 - leading], axis=-1)
    expert_out = jnp.sum(mixing[..., None] * picked, axis=1).astype(jnp.bfloat16)
    return (summed, expert_out)


def solution(mesh):
    in_specs = (
        P("ep", "tp"),
        P("ep", "tp"),
        P("ep", "tp"),
        P("tp", "ep"),
        P("tp", "ep"),
        P("tp"),
        P("tp", "ep"),
        P("tp", None),
        P(("ep", "tp"), None),
        P(),
        P(("ep", "tp"), None),
        P(("ep", "tp")),
        P(("ep", "tp")),
        P("ep", "tp", None),
        P("ep", "tp", None),
        P("ep", "tp", None),
    )
    out_specs = (P(("ep", "tp"), None), P(("ep", "tp"), None))
    return jax.shard_map(shards, mesh=mesh, in_specs=in_specs, out_specs=out_specs, check_vma=False)
```

profile of v0, /device:TPU:0, one launch (start us, length us, event | category | flops | bytes accessed | tf_op | source)
XLA Modules:
  0.0 520.2 jit_solution(1640668718798541853)
XLA Ops:
  13.5 3.3 gather_fusion
  16.9 3.1 broadcast_select_fusion
  20.0 5.6 %all-to-all-start = ((bf16[4,4,32,2048]{3,2,1,0:T(8,128)(2,1)}), bf16[4,4,32,2048]{3,2,1,0:T(8,128)(2,1)S(1)}, u32[]{:S(2)}, u32[]{:S(2)}) async-start(bf16[4,4,32,2048]{3,2,1,0:T(8,128)(2,1)} %broadcast_select_fusion), calls=%async_computation.1 | async-start | bytes 4194304 | tf_op jit(solution)/shard_map/all_to_all | solution.py:202
  29.5 3.0 fusion.52
  32.4 80.0 %custom-call.4 = f32[2,8,1,64,64]{3,4,2,1,0:T(8,128)} custom-call(f32[2,8,1,64,64]{4,3,2,1,0:T(8,128)} %fusion.52), custom_call_target="InvertDiagBlocksLowerTriangular" | custom-call | tf_op jit(solution)/shard_map/jit(_solve_triangular)/vmap(vmap())/triangular_solve | solution.py:52
  114.4 2.0 copy.100
  119.9 2.5 multiply_multiply_fusion
  125.6 2.0 fusion.50
  128.6 48.9 %while.26 = (s32[]{:T(128)}, f32[2,128,256]{2,1,0:T(8,128)S(1)}, f32[8,2,64,256]{3,2,0,1:T(8,128)}, f32[8,2]{1,0:T(8,128)}, f32[8,2,64,128]{3,2,0,1:T(8,128)}, /...) while((s32[]{:T(128)}, f32[2,128,256]{2,1,0:T(8,128)S(1)}, ...), condition=%wide.region_4.5_spmd, body=%wide.region_3.4_spmd.sunk | while | flops 176357376 | bytes 2231425 | solution.py:162
  131.0 1.8 fusion.127
  137.1 1.8 fusion.127
  143.2 1.8 fusion.127
  149.3 1.8 fusion.127
  155.4 1.8 fusion.127
  161.5 1.8 fusion.127
  167.6 1.8 fusion.127
  173.8 1.8 fusion.127
  177.6 11.2 %all-gather = f32[8,128,128]{2,1,0:T(8,128)} all-gather(f32[2,128,128]{2,1,0:T(8,128)S(1)} %get-tuple-element.243), channel_id=2, replica_groups=mesh['ep'=4,'tp'=8] {'ep'}, dimensions={0}, use_global_device_ids=true | all-gather | bytes 655360 | tf_op jit(solution)/shard_map/all_gather | solution.py:18
  188.8 11.2 %all-gather.1 = f32[8,128,128]{2,1,0:T(8,128)} all-gather(f32[2,128,128]{2,1,0:T(8,128)S(1)} %get-tuple-element.242), channel_id=3, replica_groups=mesh['ep'=4,'tp'=8] {'ep'}, dimensions={0}, use_global_device_ids=true | all-gather | bytes 655360 | tf_op jit(solution)/shard_map/all_gather | solution.py:18
  200.1 4.0 while.27
  204.1 1.8 fusion.55
  206.2 2.1 convolution_convert_fusion
  208.4 12.9 %fusion.26 = f32[4,4,32,1024]{3,2,1,0:T(8,128)} fusion(bf16[4,1024,2048]{2,1,0:T(8,128)(2,1)} %all-gather.8.cloned.1.call-done, bf16[4,4,32,2048]{3,2,1,0:T(8,128)(2,1)S(1)} %all-to-all-done), kind=kOutput, calls=%fused_computation.34 | convolution fusion | flops 2147483648 | bytes 20971520 | tf_op jit(solution)/shard_map/secd,efd->secf/dot_general | solution.py:207
  221.3 93.1 %all-gather.6.cloned.1.call-done = bf16[4,1024,2048]{2,1,0:T(8,128)(2,1)} async-done(((bf16[4,128,2048]{2,1,0:T(8,128)(2,1)}), bf16[4,1024,2048]{2,1,0:T(8,128)(2,1)}) %all-gather.6.cloned.1.call-update) | async-done | bytes 16777232 | tf_op jit(solution)/shard_map/all_gather | solution.py:203
  314.3 13.1 %fusion.36 = bf16[4,4,32,1024]{3,2,0,1:T(8,128)(2,1)} fusion(f32[4,4,32,1024]{3,2,1,0:T(8,128)} %fusion.26, bf16[4,1024,2048]{2,1,0:T(8,128)(2,1)} %all-gather.6.cloned.1.call-done, bf16[4,4,32,2048]{3,2,1,0:T(8,128)(2,1)S(1)} %all-to-all-done), kind=kOutput, calls=%fused_computation.42 | convolution fusion | flops 2150629376 | bytes 22020096 | tf_op jit(solution)/shard_map/secd,efd->secf/dot_general | solution.py:206
  327.4 137.8 %all-gather.10.cloned.1.call-done = bf16[4,1024,2048]{2,1,0:T(8,128)(2,1)} async-done(((bf16[4,128,2048]{2,1,0:T(8,128)(2,1)}), bf16[4,1024,2048]{2,1,0:T(8,128)(2,1)}) %all-gather.10.cloned.1.call-update) | async-done | bytes 16777232 | tf_op jit(solution)/shard_map/all_gather | solution.py:205
  465.3 8.5 %fusion.33 = bf16[4,4,32,2048]{3,2,0,1:T(8,128)(2,1)S(1)} fusion(bf16[4,4,32,1024]{3,2,0,1:T(8,128)(2,1)} %fusion.36, bf16[4,1024,2048]{2,1,0:T(8,128)(2,1)} %all-gather.10.cloned.1.call-done), kind=kOutput, calls=%fused_computation.40 | convolution fusion | flops 2148532224 | bytes 19922944 | tf_op jit(solution)/shard_map/secf,efd->secd/dot_general | solution.py:209
  475.3 4.0 all-to-all-start.1
  479.9 24.7 %all-to-all-done.1 = bf16[4,4,32,2048]{3,2,1,0:T(8,128)(2,1)S(1)} async-done(((bf16[4,4,32,2048]{3,2,1,0:T(8,128)(2,1)}), bf16[4,4,32,2048]{3,2,1,0:T(8,128)(2,1)S(1)}, u32[]{:S(2)}, u32[]{:S(2)}) %all-to-all-start.1) | async-done | bytes 2097184 | tf_op jit(solution)/shard_map/all_to_all | solution.py:210
  504.6 2.3 gather_fusion.1
  507.0 1.7 gather.15
  508.7 4.9 multiply_reduce_fusion
  (164 shorter events, 60.3 us)
Async XLA Ops:
  7.2 199.1 %copy-start = (bf16[256,2048]{1,0:T(8,128)(2,1)S(1)}, bf16[256,2048]{1,0:T(8,128)(2,1)}, u32[]{:S(2)}) copy-start(bf16[256,2048]{1,0:T(8,128)(2,1)} %param.27) | copy-start | bytes 3145732
  7.2 201.2 %all-gather.8.cloned.1.call-start = ((), (), s32[]{:S(2)}) async-start(), calls=%async_computation.5 | async-start | bytes 18874368 | tf_op jit(solution)/shard_map/all_gather | solution.py:204
  7.9 1.5 copy-start.11
  7.9 5.2 %copy-start.2 = (bf16[128,2048]{1,0:T(8,128)(2,1)S(1)}, bf16[128,2048]{1,0:T(8,128)(2,1)}, u32[]{:S(2)}) copy-start(bf16[128,2048]{1,0:T(8,128)(2,1)} %param.28) | copy-start | bytes 1572868
  7.9 5.4 %copy-start.14 = (f32[2048]{0:T(1024)S(1)}, f32[2048]{0:T(1024)}, u32[]{:S(2)}) copy-start(f32[2048]{0:T(1024)} %param.29) | copy-start | bytes 24580
  7.9 306.4 %all-gather.6.cloned.1.call-start = ((), (), s32[]{:S(2)}) async-start(), calls=%async_computation.4 | async-start | bytes 18874368 | tf_op jit(solution)/shard_map/all_gather | solution.py:203
  8.7 456.6 %all-gather.10.cloned.1.call-start = ((), (), s32[]{:S(2)}) async-start(), calls=%async_computation.6 | async-start | bytes 18874368 | tf_op jit(solution)/shard_map/all_gather | solution.py:205
  11.0 0.6 copy-start.9
  11.6 1.5 copy-start.17
  20.0 5.6 %copy-start.23 = (f32[2]{0:T(128)S(1)}, f32[2]{0:T(128)}, u32[]{:S(2)}) copy-start(f32[2]{0:T(128)} %param.25) | copy-start | bytes 28
  20.0 5.6 %copy-start.19 = (f32[2,512]{1,0:T(2,128)S(1)}, f32[2,512]{1,0:T(2,128)}, u32[]{:S(2)}) copy-start(f32[2,512]{1,0:T(2,128)} %param.26) | copy-start | bytes 12292
  20.0 5.6 %copy-start.20 = (bf16[2,512]{1,0:T(2,128)(2,1)S(1)}, bf16[2,512]{1,0:T(2,128)(2,1)}, u32[]{:S(2)}) copy-start(bf16[2,512]{1,0:T(2,128)(2,1)} %param.24) | copy-start | bytes 6148
  20.0 5.8 %copy-start.6 = (bf16[512,256]{1,0:T(8,128)(2,1)S(1)}, bf16[512,256]{1,0:T(8,128)(2,1)}, u32[]{:S(2)}) copy-start(bf16[512,256]{1,0:T(8,128)(2,1)} %param.21) | copy-start | bytes 786436
  20.0 188.4 %all-to-all-start = ((bf16[4,4,32,2048]{3,2,1,0:T(8,128)(2,1)}), bf16[4,4,32,2048]{3,2,1,0:T(8,128)(2,1)S(1)}, u32[]{:S(2)}, u32[]{:S(2)}) async-start(bf16[4,4,32,2048]{3,2,1,0:T(8,128)(2,1)} %broadcast_select_fusion), calls=%async_computation.1 | async-start | bytes 4194304 | tf_op jit(solution)/shard_map/all_to_all | solution.py:202
  25.6 488.0 %reduce-scatter.2.cloned.1.call-start = ((), (), s32[]{:S(2)}) async-start(), calls=%async_computation.3 | async-start | bytes 2359296 | tf_op jit(solution)/shard_map/reduce_scatter | solution.py:178
  28.6 0.6 copy-start.15
  28.7 0.8 copy-start.4
  116.8 0.6 copy-start.13
  118.1 4.3 copy-start.7
  122.4 2.0 copy-start.3
  122.4 3.1 copy-start.5
  122.4 3.1 copy-start.8
  122.4 3.1 copy-start.16
  123.6 4.0 copy-start.21
  475.3 4.0 copy-start.10
  475.3 4.2 copy-start.12
  475.3 4.4 copy-start.24
  475.3 4.4 copy-start.22
  475.3 4.6 copy-start.18
  475.3 29.3 %all-to-all-start.1 = ((bf16[4,4,32,2048]{3,2,1,0:T(8,128)(2,1)}), bf16[4,4,32,2048]{3,2,1,0:T(8,128)(2,1)S(1)}, u32[]{:S(2)}, u32[]{:S(2)}) async-start(bf16[4,4,32,2048]{3,2,1,0:T(8,128)(2,1)} %copy.119), calls=%async_computation.2 | async-start | bytes 4194304 | tf_op jit(solution)/shard_map/all_to_all | solution.py:210
  504.6 9.0 %copy-start.1 = (bf16[256,2048]{1,0:T(8,128)(2,1)S(1)}, bf16[256,2048]{1,0:T(8,128)(2,1)}, u32[]{:S(2)}) copy-start(bf16[256,2048]{1,0:T(8,128)(2,1)} %param.27) | copy-start | bytes 3145732
Sparse Core Ops, SparseCore 0:
  9.6 153.7 all-gather.7
  165.0 149.2 all-gather.5
  316.0 149.2 all-gather.9
  468.0 34.1 reduce-scatter.1
where the time goes:
time: 522 us; the launch traced here: 520 us
  waiting for transfers between devices  258 us (49%)
  other arithmetic  98.3 us (19%)
  matrix products  91.2 us (17%)
  local copies, waits for them, and re-layouts  26 us (5%)
  blocking collectives  22.5 us (4%)
  between operations  14.2 us (3%)
  starting transfers between devices  9.7 us (2%)
    all_gather x1, waiting for transfers between devices, shards(): down_piece = lax.all_gather(expert_down_weight, 'tp', axis=1, tiled=True)  138 us
    all_gather x1, waiting for transfers between devices, shards(): gate_piece = lax.all_gather(expert_gate_weight, 'tp', axis=1, tiled=True)  93.1 us
    another operation x2, other arithmetic, block_terms(): jax.scipy.linalg.solve_triangular(system, rhs_cols, lower=True, unit_diag...  80 us
    all_to_all x1, waiting for transfers between devices, shards(): lax.all_to_all(produced.astype(jnp.bfloat16), 'ep', split_axis=0, concat_...  24.7 us
    all_gather x2, blocking collectives, prefix(): pieces = jax.tree.map(lambda part: lax.all_gather(part, axis), value)  22.5 us
    dot_general x8, matrix products, carry_step(): jnp.einsum('hcj,hjv->hcv', scores, value_updates, precision=precise_setting)  14.2 us
    dot_general x1, matrix products, shards(): jnp.einsum('secd,efd->secf', arrived, gate_piece, preferred_element_type=...  13.1 us
    dot_general x1, matrix products, shards(): jnp.einsum('secd,efd->secf', arrived, up_piece, preferred_element_type=jn...  12.9 us
  transfers between devices with their start and end apart: 6, of which 3 were waited for; matrix products, arithmetic and copies ran while one was open for 41% of the time, Pallas kernels for 0%

commit v1 on v0

--- a/solution.py
+++ b/solution.py
@@ -202,11 +202,41 @@
     arrived = lax.all_to_all(outgoing, "ep", split_axis=0, concat_axis=0, tiled=True)
     gate_piece = lax.all_gather(expert_gate_weight, "tp", axis=1, tiled=True)
     up_piece = lax.all_gather(expert_up_weight, "tp", axis=1, tiled=True)
-    down_piece = lax.all_gather(expert_down_weight, "tp", axis=1, tiled=True)
     gating = jnp.einsum("secd,efd->secf", arrived, gate_piece, preferred_element_type=jnp.float32)
     upward = jnp.einsum("secd,efd->secf", arrived, up_piece, preferred_element_type=jnp.float32)
     hidden = (jax.nn.silu(gating) * upward).astype(jnp.bfloat16)
-    produced = jnp.einsum("secf,efd->secd", hidden, down_piece, preferred_element_type=jnp.float32)
+    size, index, span = (lax.axis_size("tp"), lax.axis_index("tp"), expert_down_weight.shape[1])
+    right = [(i, (i + 1) % size) for i in range(size)]
+    left = [(i, (i - 1) % size) for i in range(size)]
+    halfway = size // 2
+    from_left = from_right = expert_down_weight
+    so_far = jnp.einsum(
+        "secf,efd->secd",
+        lax.dynamic_slice_in_dim(hidden, index * span, expert_down_weight.shape[1], axis=3),
+        expert_down_weight,
+        preferred_element_type=jnp.float32,
+    )
+    for hop in range(1, halfway + 1):
+        from_left = lax.ppermute(from_left, "tp", right)
+        if hop < size - halfway:
+            from_right = lax.ppermute(from_right, "tp", left)
+            so_far = so_far + jnp.einsum(
+                "secf,efd->secd",
+                lax.dynamic_slice_in_dim(
+                    hidden, (index + hop) % size * span, from_right.shape[1], axis=3
+                ),
+                from_right,
+                preferred_element_type=jnp.float32,
+            )
+        so_far = so_far + jnp.einsum(
+            "secf,efd->secd",
+            lax.dynamic_slice_in_dim(
+                hidden, (index - hop) % size * span, from_left.shape[1], axis=3
+            ),
+            from_left,
+            preferred_element_type=jnp.float32,
+        )
+    produced = so_far
     returned = lax.all_to_all(
         produced.astype(jnp.bfloat16), "ep", split_axis=0, concat_axis=0, tiled=True
     )

time: 522 us -> 546 us (1.046)
  starting transfers between devices: 9.7 us -> 54.3 us
  waiting for transfers between devices: 258 us -> 222 us
  matrix products: 91.2 us -> 112 us
  local copies, waits for them, and re-layouts: 26 us -> 19 us
    all_gather x1 -> x0, waiting for transfers between devices: 138 us -> none  [shards(): down_piece = lax.all_gather(expert_down_weight, 'tp', axis=1, tiled=True)]
    ppermute x0 -> x7, waiting for transfers between devices: none -> 53.4 us  [the longest x4 53.4 us: shards(): from_left = lax.ppermute(from_left, 'tp', right)]
    all_gather x1, waiting for transfers between devices: 93.1 us -> 142 us  [shards(): gate_piece = lax.all_gather(expert_gate_weight, 'tp', axis=1, tiled=True)]
    ppermute x0 -> x7, starting transfers between devices: none -> 46.2 us  [the longest x3 45 us: shards(): from_right = lax.ppermute(from_right, 'tp', left)]
    dot_general x1 -> x8, matrix products: 8.46 us -> 31.4 us  [the longest x4 18 us: shards(): jnp.einsum('secf,efd->secd', lax.dynamic_slice_in_dim(hidden, (index - ho...]
    mul x8, local copies, waits for them, and re-layouts: 5.52 us -> 0.04 us  [carry_step(): recurrent_state * block_retention[:, None, None]]
  transfers between devices with their start and end apart: 6 -> 12, of which waited for: 3 -> 3; matrix products, arithmetic and copies ran while one was open for 41% -> 42% of each run, Pallas kernels for 0% -> 0%
where the time goes in v1:
time: 546 us; the launch traced here: 543 us
  waiting for transfers between devices  222 us (41%)
  matrix products  112 us (21%)
  other arithmetic  98.2 us (18%)
  starting transfers between devices  54.3 us (10%)
  blocking collectives  23.6 us (4%)
  local copies, waits for them, and re-layouts  19 us (3%)
  between operations  14.3 us (3%)
    all_gather x1, waiting for transfers between devices, shards(): gate_piece = lax.all_gather(expert_gate_weight, 'tp', axis=1, tiled=True)  142 us
    another operation x2, other arithmetic, block_terms(): jax.scipy.linalg.solve_triangular(system, rhs_cols, lower=True, unit_diag...  80 us
    ppermute x4, waiting for transfers between devices, shards(): from_left = lax.ppermute(from_left, 'tp', right)  53.4 us
    ppermute x3, starting transfers between devices, shards(): from_right = lax.ppermute(from_right, 'tp', left)  45 us
    all_to_all x1, waiting for transfers between devices, shards(): lax.all_to_all(produced.astype(jnp.bfloat16), 'ep', split_axis=0, concat_...  24.9 us
    all_gather x2, blocking collectives, prefix(): pieces = jax.tree.map(lambda part: lax.all_gather(part, axis), value)  23.6 us
    dot_general x4, matrix products, shards(): jnp.einsum('secf,efd->secd', lax.dynamic_slice_in_dim(hidden, (index - ho...  18 us
    dot_general x8, matrix products, carry_step(): jnp.einsum('hcj,hjv->hcv', scores, value_updates, precision=precise_setting)  14.1 us
  transfers between devices with their start and end apart: 12, of which 3 were waited for; matrix products, arithmetic and copies ran while one was open for 42% of the time, Pallas kernels for 0%

profile of v1, /device:TPU:0, one launch (start us, length us, event | category | flops | bytes accessed | tf_op | source)
XLA Modules:
  0.0 543.4 jit_solution(2958217090373059836)
XLA Ops:
  9.2 4.1 collective-permute-start
  16.9 3.3 gather_fusion
  20.1 3.4 broadcast_select_fusion
  23.6 4.3 all-to-all-start
  31.4 2.2 fusion.60
  34.5 53.4 %collective-permute-done.1 = bf16[4,128,2048]{2,1,0:T(8,128)(2,1)} collective-permute-done((bf16[4,128,2048]{2,1,0:T(8,128)(2,1)}, bf16[4,128,2048]{2,1,0:T(8,128)(2,1)}, u32[]{:S(2)}, u32[]{:S(2)}) %collective-permute-start.1) | collective-permute-done | bytes 2097184 | tf_op jit(solution)/shard_map/ppermute | solution.py:220
  88.6 80.0 %custom-call.4 = f32[2,8,1,64,64]{3,4,2,1,0:T(8,128)} custom-call(f32[2,8,1,64,64]{4,3,2,1,0:T(8,128)} %fusion.60), custom_call_target="InvertDiagBlocksLowerTriangular" | custom-call | tf_op jit(solution)/shard_map/jit(_solve_triangular)/vmap(vmap())/triangular_solve | solution.py:52
  168.6 2.1 copy.100
  172.0 2.5 multiply_multiply_fusion
  180.6 2.8 collective-permute-start.2
  183.5 43.3 %while.26 = (s32[]{:T(128)}, f32[2,128,256]{2,1,0:T(8,128)S(1)}, f32[8,2,64,256]{3,2,0,1:T(8,128)}, f32[8,2]{1,0:T(8,128)S(1)}, f32[8,2,64,128]{3,2,0,1:T(8,128)...) while((s32[]{:T(128)}, f32[2,128,256]{2,1,0:T(8,128)S(1)}, ...), condition=%wide.region_4.5_spmd, body=%wide.region_3.4_spmd.sunk | while | flops 176357376 | bytes 2231425 | solution.py:162
  227.5 13.8 %all-gather = f32[8,128,128]{2,1,0:T(8,128)} all-gather(f32[2,128,128]{2,1,0:T(8,128)} %get-tuple-element.243), channel_id=2, replica_groups=mesh['ep'=4,'tp'=8] {'ep'}, dimensions={0}, use_global_device_ids=true | all-gather | bytes 655360 | tf_op jit(solution)/shard_map/all_gather | solution.py:18
  241.3 9.8 %all-gather.1 = f32[8,128,128]{2,1,0:T(8,128)} all-gather(f32[2,128,128]{2,1,0:T(8,128)S(1)} %get-tuple-element.242), channel_id=3, replica_groups=mesh['ep'=4,'tp'=8] {'ep'}, dimensions={0}, use_global_device_ids=true | all-gather | bytes 655360 | tf_op jit(solution)/shard_map/all_gather | solution.py:18
  251.1 3.9 while.27
  257.0 2.1 convolution_convert_fusion
  259.3 38.0 %collective-permute-start.4 = (bf16[4,128,2048]{2,1,0:T(8,128)(2,1)}, bf16[4,128,2048]{2,1,0:T(8,128)(2,1)}, u32[]{:S(2)}, u32[]{:S(2)}) collective-permute-start(bf16[4,128,2048]{2,1,0:T(8,128)(2,1)} %collective-permute-done.2), channel_id=1, source_target_pairs={{0,7},{1,0},{2,1},{3,2},{4,3},{5,4},{6,5},{7,6},{8,15},{9,8},{10,9... | collective-permute-start | bytes 6291464 | tf_op jit(solution)/shard_map/ppermute | solution.py:222
  297.4 12.7 %fusion.24 = f32[4,4,32,1024]{3,2,1,0:T(8,128)} fusion(bf16[4,1024,2048]{2,1,0:T(8,128)(2,1)} %all-gather.7.cloned.1.call-done, bf16[4,4,32,2048]{3,2,1,0:T(8,128)(2,1)S(1)} %all-to-all-done), kind=kOutput, calls=%fused_computation.32 | convolution fusion | flops 2147483648 | bytes 20971520 | tf_op jit(solution)/shard_map/secd,efd->secf/dot_general | solution.py:206
  310.1 141.9 %all-gather.5.cloned.1.call-done = bf16[4,1024,2048]{2,1,0:T(8,128)(2,1)} async-done(((bf16[4,128,2048]{2,1,0:T(8,128)(2,1)}), bf16[4,1024,2048]{2,1,0:T(8,128)(2,1)}) %all-gather.5.cloned.1.call-update) | async-done | bytes 16777232 | tf_op jit(solution)/shard_map/all_gather | solution.py:203
  452.0 12.1 %fusion.44 = bf16[4,4,32,1024]{3,2,0,1:T(8,128)(2,1)S(1)} fusion(f32[4,4,32,1024]{3,2,1,0:T(8,128)} %fusion.24, bf16[4,1024,2048]{2,1,0:T(8,128)(2,1)} %all-gather.5.cloned.1.call-done, bf16[4,4,32,2048]{3,2,1,0:T(8,128)(2,1)S(1)} %all-to-all-done), kind=kOutput, calls=%fused_computation.55 | convolution fusion | flops 2150629376 | bytes 22020096 | tf_op jit(solution)/shard_map/secd,efd->secf/dot_general | solution.py:205
  464.0 2.3 fusion.42
  466.3 2.3 fusion.30
  468.6 2.3 fusion.34
  471.0 2.3 fusion.36
  473.3 4.3 fusion.38
  477.5 4.3 fusion.40
  481.8 4.5 fusion.32
  486.4 9.1 %fusion.28 = bf16[4,4,32,2048]{3,2,0,1:T(8,128)(2,1)} fusion(f32[4,4,32,2048]{3,2,1,0:T(8,128)S(1)} %fusion.30, f32[4,4,32,2048]{3,2,1,0:T(8,128)} %fusion.32, f32[4,4,32,2048]{3,2,1,0:T(8,128)S(1)} %fusion.34, f32[4,4,32,2048]{3,2,1,0:T(8,128)S(1)} %fusion.36, f32[4,4,32,2048]{3,2,1,0:T(8,128)} %fusion.38, f32[4,4,32,2048]{3,2,1,0:T(8,128)S(1)} %fusion.42, ...), kind=kOutput, calls=%fused_computation.38 | convolution fusion | flops 276824064 | bytes 33685508 | tf_op jit(solution)/shard_map/secf,efd->secd/dot_general | solution.py:231
  495.5 3.2 copy.119
  498.7 3.7 all-to-all-start.1
  503.0 24.9 %all-to-all-done.1 = bf16[4,4,32,2048]{3,2,1,0:T(8,128)(2,1)S(1)} async-done(((bf16[4,4,32,2048]{3,2,1,0:T(8,128)(2,1)}), bf16[4,4,32,2048]{3,2,1,0:T(8,128)(2,1)S(1)}, u32[]{:S(2)}, u32[]{:S(2)}) %all-to-all-start.1) | async-done | bytes 2097184 | tf_op jit(solution)/shard_map/all_to_all | solution.py:240
  527.9 2.3 gather_fusion.1
  532.0 4.9 multiply_reduce_fusion
  (166 shorter events, 69.8 us)
Async XLA Ops:
  7.2 249.9 %copy-start = (bf16[256,2048]{1,0:T(8,128)(2,1)S(1)}, bf16[256,2048]{1,0:T(8,128)(2,1)}, u32[]{:S(2)}) copy-start(bf16[256,2048]{1,0:T(8,128)(2,1)} %param.27) | copy-start | bytes 3145732
  7.2 6.2 %copy-start.8 = (s32[128,2]{0,1:T(2,128)S(1)}, s32[128,2]{0,1:T(2,128)}, u32[]{:S(2)}) copy-start(s32[128,2]{0,1:T(2,128)} %param.30) | copy-start | bytes 3076
  7.2 9.3 %copy-start.2 = (bf16[128,2048]{1,0:T(8,128)(2,1)S(1)}, bf16[128,2048]{1,0:T(8,128)(2,1)}, u32[]{:S(2)}) copy-start(bf16[128,2048]{1,0:T(8,128)(2,1)} %param.28) | copy-start | bytes 1572868
  7.2 9.5 %copy-start.9 = (f32[2048]{0:T(1024)S(1)}, f32[2048]{0:T(1024)}, u32[]{:S(2)}) copy-start(f32[2048]{0:T(1024)} %param.29) | copy-start | bytes 24580
  7.2 290.1 %all-gather.7.cloned.1.call-start = ((), (), s32[]{:S(2)}) async-start(), calls=%async_computation.5 | async-start | bytes 18874368 | tf_op jit(solution)/shard_map/all_gather | solution.py:204
  7.9 444.0 %all-gather.5.cloned.1.call-start = ((), (), s32[]{:S(2)}) async-start(), calls=%async_computation.4 | async-start | bytes 18874368 | tf_op jit(solution)/shard_map/all_gather | solution.py:203
  8.7 79.2 %collective-permute-start.1 = (bf16[4,128,2048]{2,1,0:T(8,128)(2,1)}, bf16[4,128,2048]{2,1,0:T(8,128)(2,1)}, u32[]{:S(2)}, u32[]{:S(2)}) collective-permute-start(bf16[4,128,2048]{2,1,0:T(8,128)(2,1)} %param.35), channel_id=1, source_target_pairs={{0,1},{1,2},{2,3},{3,4},{4,5},{5,6},{6,7},{7,0},{8,9},{9,10},{10,1... | collective-permute-start | bytes 6291464 | tf_op jit(solution)/shard_map/ppermute | solution.py:220
  9.2 171.4 %collective-permute-start = (bf16[4,128,2048]{2,1,0:T(8,128)(2,1)}, bf16[4,128,2048]{2,1,0:T(8,128)(2,1)}, u32[]{:S(2)}, u32[]{:S(2)}) collective-permute-start(bf16[4,128,2048]{2,1,0:T(8,128)(2,1)} %param.35), channel_id=1, source_target_pairs={{0,7},{1,0},{2,1},{3,2},{4,3},{5,4},{6,5},{7,6},{8,15},{9,8},{10,9... | collective-permute-start | bytes 6291464 | tf_op jit(solution)/shard_map/ppermute | solution.py:222
  23.6 4.3 copy-start.6
  23.6 4.6 copy-start.15
  23.6 4.6 copy-start.10
  23.6 4.6 copy-start.12
  23.6 4.8 copy-start.11
  23.6 273.7 %all-to-all-start = ((bf16[4,4,32,2048]{3,2,1,0:T(8,128)(2,1)}), bf16[4,4,32,2048]{3,2,1,0:T(8,128)(2,1)S(1)}, u32[]{:S(2)}, u32[]{:S(2)}) async-start(bf16[4,4,32,2048]{3,2,1,0:T(8,128)(2,1)} %broadcast_select_fusion), calls=%async_computation.1 | async-start | bytes 4194304 | tf_op jit(solution)/shard_map/all_to_all | solution.py:202
  27.9 509.0 %reduce-scatter.2.cloned.1.call-start = ((), (), s32[]{:S(2)}) async-start(), calls=%async_computation.3 | async-start | bytes 2359296 | tf_op jit(solution)/shard_map/reduce_scatter | solution.py:178
  31.4 3.1 copy-start.4
  87.9 95.6 %collective-permute-start.3 = (bf16[4,128,2048]{2,1,0:T(8,128)(2,1)}, bf16[4,128,2048]{2,1,0:T(8,128)(2,1)}, u32[]{:S(2)}, u32[]{:S(2)}) collective-permute-start(bf16[4,128,2048]{2,1,0:T(8,128)(2,1)} %collective-permute-done.1), channel_id=1, source_target_pairs={{0,1},{1,2},{2,3},{3,4},{4,5},{5,6},{6,7},{7,0},{8,9},{9,10},{10,1... | collective-permute-start | bytes 6291464 | tf_op jit(solution)/shard_map/ppermute | solution.py:220
  170.8 3.6 copy-start.7
  174.4 2.0 copy-start.3
  174.4 3.2 copy-start.5
  175.5 4.0 copy-start.13
  180.6 78.6 %collective-permute-start.2 = (bf16[4,128,2048]{2,1,0:T(8,128)(2,1)}, bf16[4,128,2048]{2,1,0:T(8,128)(2,1)}, u32[]{:S(2)}, u32[]{:S(2)}) collective-permute-start(bf16[4,128,2048]{2,1,0:T(8,128)(2,1)} %collective-permute-done), channel_id=1, source_target_pairs={{0,7},{1,0},{2,1},{3,2},{4,3},{5,4},{6,5},{7,6},{8,15},{9,8},{10,9... | collective-permute-start | bytes 6291464 | tf_op jit(solution)/shard_map/ppermute | solution.py:222
  183.5 113.8 %collective-permute-start.5 = (bf16[4,128,2048]{2,1,0:T(8,128)(2,1)}, bf16[4,128,2048]{2,1,0:T(8,128)(2,1)}, u32[]{:S(2)}, u32[]{:S(2)}) collective-permute-start(bf16[4,128,2048]{2,1,0:T(8,128)(2,1)} %collective-permute-done.3), channel_id=1, source_target_pairs={{0,1},{1,2},{2,3},{3,4},{4,5},{5,6},{6,7},{7,0},{8,9},{9,10},{10,1... | collective-permute-start | bytes 6291464 | tf_op jit(solution)/shard_map/ppermute | solution.py:220
  259.3 222.6 %collective-permute-start.4 = (bf16[4,128,2048]{2,1,0:T(8,128)(2,1)}, bf16[4,128,2048]{2,1,0:T(8,128)(2,1)}, u32[]{:S(2)}, u32[]{:S(2)}) collective-permute-start(bf16[4,128,2048]{2,1,0:T(8,128)(2,1)} %collective-permute-done.2), channel_id=1, source_target_pairs={{0,7},{1,0},{2,1},{3,2},{4,3},{5,4},{6,5},{7,6},{8,15},{9,8},{10,9... | collective-permute-start | bytes 6291464 | tf_op jit(solution)/shard_map/ppermute | solution.py:222
  297.3 189.0 %collective-permute-start.6 = (bf16[4,128,2048]{2,1,0:T(8,128)(2,1)}, bf16[4,128,2048]{2,1,0:T(8,128)(2,1)}, u32[]{:S(2)}, u32[]{:S(2)}) collective-permute-start(bf16[4,128,2048]{2,1,0:T(8,128)(2,1)} %collective-permute-done.5), channel_id=1, source_target_pairs={{0,1},{1,2},{2,3},{3,4},{4,5},{5,6},{6,7},{7,0},{8,9},{9,10},{10,1... | collective-permute-start | bytes 6291464 | tf_op jit(solution)/shard_map/ppermute | solution.py:220
  498.7 4.1 copy-start.16
  498.7 4.1 copy-start.14
  498.7 29.2 %all-to-all-start.1 = ((bf16[4,4,32,2048]{3,2,1,0:T(8,128)(2,1)}), bf16[4,4,32,2048]{3,2,1,0:T(8,128)(2,1)S(1)}, u32[]{:S(2)}, u32[]{:S(2)}) async-start(bf16[4,4,32,2048]{3,2,1,0:T(8,128)(2,1)} %copy.119), calls=%async_computation.2 | async-start | bytes 4194304 | tf_op jit(solution)/shard_map/all_to_all | solution.py:240
  527.9 9.0 %copy-start.1 = (bf16[256,2048]{1,0:T(8,128)(2,1)S(1)}, bf16[256,2048]{1,0:T(8,128)(2,1)}, u32[]{:S(2)}) copy-start(bf16[256,2048]{1,0:T(8,128)(2,1)} %param.27) | copy-start | bytes 3145732
Sparse Core Ops, SparseCore 0:
  9.6 225.9 all-gather.6
  237.3 214.6 all-gather.4
  454.8 36.1 reduce-scatter.1
